TPU v7x, 32 devices: a whole 2x2x4 slice. The times are simulated.
32 devices in a mesh: ep: 8 (over z, x), tp: 4 (over y, core).
Axes of the slice: x: 2, y: 2, z: 4, core: 2. Of those that a mesh axis runs over, the one named last changes fastest.
Arguments:
- tokens: bfloat16 [128, 2048], P('ep'), may hold values from -120 to 120
- lengths: int32 [128], P('ep'), may hold values from 1 to 768, as said below
- cache_kv: bfloat16 [128, 768, 16, 128], P('ep', None, 'tp'), may hold values from -64 to 64
- cache_cum: float32 [128, 16, 768], P('ep', 'tp'), may hold values from -768 to 0, as said below
- norm_attn: float32 [2048], replicated, may hold values from 0.1 to 1.9
- w_query: bfloat16 [2048, 1024], P(None, 'tp'), may hold values from -0.125 to 0.125
- w_key: bfloat16 [2048, 1024], P(None, 'tp'), may hold values from -0.125 to 0.125
- w_value: bfloat16 [2048, 1024], P(None, 'tp'), may hold values from -0.125 to 0.125
- w_forget: bfloat16 [2048, 16], P(None, 'tp'), may hold values from -0.125 to 0.125
- b_forget: float32 [16], P('tp'), may hold values from -1 to 2
- w_output: bfloat16 [1024, 2048], P('tp'), may hold values from -0.1875 to 0.1875
- norm_ffn: float32 [2048], replicated, may hold values from 0.1 to 1.9
- shared_gate: bfloat16 [2048, 512], P(None, 'tp'), may hold values from -0.125 to 0.125
- shared_up: bfloat16 [2048, 512], P(None, 'tp'), may hold values from -0.125 to 0.125
- shared_down: bfloat16 [512, 2048], P('tp'), may hold values from -0.25 to 0.25
- expert_gate: bfloat16 [24, 2048, 512], P('ep', None, 'tp'), may hold values from -0.125 to 0.125
- expert_up: bfloat16 [24, 2048, 512], P('ep', None, 'tp'), may hold values from -0.125 to 0.125
- expert_down: bfloat16 [24, 512, 2048], P('ep', 'tp'), may hold values from -0.25 to 0.25
- route_ids: int32 [128, 6], P('ep'), may hold values from 0 to 23, all different within a row; in each aligned block of 16 rows (0 to 15, 16 to 31, ...) at most 8 rows name the same one
- route_weight: float32 [128, 6], P('ep'), may hold values from 0.1 to 0.8
Outputs:
- output: bfloat16 [128, 2048], P('ep', 'tp')
- new_kv: bfloat16 [128, 16, 128], P('ep', 'tp')
- new_cum: float32 [128, 16], P('ep', 'tp')
Inputs may be any that keep to these rules, and one draw needn't show every extreme that they name: `lengths`: every block of 16 sequences of one index of ep holds one with 768. `route_ids`: in the rows of one device (aligned blocks of 16 rows) no expert is named more than 8 times. `cache_cum`: Non-increasing along positions.
All inputs are finite; a program needn't handle non-finite values.
Results may differ from a plain program's by a relative error of at most 0.012.
Values may be sent and summed in bfloat16 or wider, within the bound.
A program may use at most 128 MiB of HBM per device.

v0:
```python
import jax
import jax.numpy as jnp
from jax import lax
from jax.sharding import PartitionSpec as P

HEAD_DIM = 64
epsilon = 1e-06


def rms_scale(row_block, gain):
    widened = row_block.astype(jnp.float32)
    return widened * lax.rsqrt(jnp.mean(widened * widened, axis=-1, keepdims=True) + epsilon) * gain


def shards(
    tokens,
    lengths,
    cache_kv,
    cache_cum,
    norm_attn,
    w_query,
    w_key,
    w_value,
    w_forget,
    b_forget,
    w_output,
    norm_ffn,
    shared_gate,
    shared_up,
    shared_down,
    expert_gate,
    expert_up,
    expert_down,
    route_ids,
    route_weight,
):
    ep_size = lax.axis_size("ep")
    tp_size = lax.axis_size("tp")
    tp_place = lax.axis_index("tp")
    seq_dev, model_width = tokens.shape
    width_part = model_width // tp_size
    heads_here = w_query.shape[1] // HEAD_DIM
    cache_len = cache_kv.shape[1]
    score_scale = HEAD_DIM ** (-0.5)
    normed = rms_scale(tokens, norm_attn).astype(jnp.bfloat16)
    queries = (
        jnp.dot(normed, w_query, preferred_element_type=jnp.float32)
        .astype(jnp.bfloat16)
        .reshape(seq_dev, heads_here, HEAD_DIM)
    )
    key_new = (
        jnp.dot(normed, w_key, preferred_element_type=jnp.float32)
        .astype(jnp.bfloat16)
        .reshape(seq_dev, heads_here, HEAD_DIM)
    )
    value_new = (
        jnp.dot(normed, w_value, preferred_element_type=jnp.float32)
        .astype(jnp.bfloat16)
        .reshape(seq_dev, heads_here, HEAD_DIM)
    )
    forget_log = jax.nn.log_sigmoid(
        jnp.dot(normed, w_forget, preferred_element_type=jnp.float32) + b_forget
    )
    last_index = jnp.broadcast_to((lengths - 1)[:, None, None], (seq_dev, heads_here, 1))
    cum_new = jnp.take_along_axis(cache_cum, last_index, axis=2)[:, :, 0] + forget_log
    past_scores = (
        jnp.einsum(
            "shd,slhd->shl",
            queries,
            cache_kv[:, :, :, :HEAD_DIM],
            preferred_element_type=jnp.float32,
        )
        * score_scale
    )
    past_scores = past_scores + cum_new[:, :, None] - cache_cum
    is_valid = jnp.arange(cache_len, dtype=jnp.int32)[None, None, :] < lengths[:, None, None]
    past_scores = jnp.where(is_valid, past_scores, -jnp.inf)
    own_score = (
        jnp.sum(queries.astype(jnp.float32) * key_new.astype(jnp.float32), axis=2) * score_scale
    )
    row_max = jnp.maximum(jnp.max(past_scores, axis=2), own_score)
    weights_past = jnp.exp(past_scores - row_max[:, :, None])
    weight_own = jnp.exp(own_score - row_max)
    weight_sum = jnp.sum(weights_past, axis=2) + weight_own
    probs_past = (weights_past / weight_sum[:, :, None]).astype(jnp.bfloat16)
    prob_own = (weight_own / weight_sum).astype(jnp.bfloat16)
    mixed = jnp.einsum(
        "shl,slhd->shd",
        probs_past,
        cache_kv[:, :, :, HEAD_DIM:],
        preferred_element_type=jnp.float32,
    )
    mixed = mixed + prob_own.astype(jnp.float32)[:, :, None] * value_new.astype(jnp.float32)
    attended = mixed.astype(jnp.bfloat16).reshape(seq_dev, heads_here * HEAD_DIM)
    partial_value = jnp.dot(attended, w_output, preferred_element_type=jnp.float32)
    summed = lax.psum(partial_value.astype(jnp.bfloat16), "tp").astype(jnp.float32)
    residual = (tokens.astype(jnp.float32) + summed).astype(jnp.bfloat16)
    ffn_in = rms_scale(residual, norm_ffn).astype(jnp.bfloat16)
    residual_part = lax.dynamic_slice_in_dim(residual, tp_place * width_part, width_part, 1)
    shared_hidden = (
        jax.nn.silu(jnp.dot(ffn_in, shared_gate, preferred_element_type=jnp.float32))
        * jnp.dot(ffn_in, shared_up, preferred_element_type=jnp.float32)
    ).astype(jnp.bfloat16)
    shared_part = jnp.dot(shared_hidden, shared_down, preferred_element_type=jnp.float32).astype(
        jnp.bfloat16
    )
    top_count = route_ids.shape[1]
    experts_here = expert_gate.shape[0]
    experts_all = experts_here * ep_size
    capacity = max(2, 2 * (seq_dev * top_count // experts_all))
    slot_count = experts_all * capacity
    route_flat = route_ids.reshape(-1)
    onehot = (route_flat[:, None] == jnp.arange(experts_all, dtype=jnp.int32)[None, :]).astype(
        jnp.int32
    )
    before = jnp.cumsum(onehot, axis=0) - onehot
    slot_rank = jnp.sum(before * onehot, axis=1)
    owner_index = route_flat // experts_here
    slot_local = route_flat % experts_here
    slot_index = ((slot_local * ep_size + owner_index) * capacity + slot_rank).reshape(
        seq_dev, top_count
    )
    slot_ids = jnp.arange(slot_count, dtype=jnp.int32)
    picker = jnp.sum(
        (slot_ids[:, None, None] == slot_index[None, :, :]).astype(jnp.bfloat16), axis=2
    )
    combine = jnp.sum(
        jnp.where(slot_ids[None, None, :] == slot_index[:, :, None], route_weight[:, :, None], 0.0),
        axis=1,
    )
    own_part = lax.dynamic_slice_in_dim(ffn_in, tp_place * width_part, width_part, 1)
    chosen = jnp.dot(picker, own_part, preferred_element_type=jnp.float32).astype(jnp.bfloat16)
    moved = lax.all_to_all(
        chosen.reshape(experts_here, ep_size, capacity, width_part),
        "ep",
        split_axis=1,
        concat_axis=1,
        tiled=True,
    )
    arrived = lax.all_gather(moved, "tp", axis=3, tiled=True)
    row_count = ep_size * capacity
    arrived = arrived.reshape(experts_here, row_count, model_width)
    gate_value = jnp.einsum(
        "erd,edf->erf", arrived, expert_gate, preferred_element_type=jnp.float32
    )
    up_value = jnp.einsum("erd,edf->erf", arrived, expert_up, preferred_element_type=jnp.float32)
    expert_hidden = (jax.nn.silu(gate_value) * up_value).astype(jnp.bfloat16)
    expert_part = jnp.einsum(
        "erf,efd->erd", expert_hidden, expert_down, preferred_element_type=jnp.float32
    ).astype(jnp.bfloat16)
    expert_pieces, shared_pieces = (
        lax.all_to_all(
            expert_part.reshape(experts_here, row_count, tp_size, width_part),
            "tp",
            split_axis=2,
            concat_axis=2,
            tiled=True,
        ),
        lax.all_to_all(
            shared_part.reshape(1, seq_dev, tp_size, width_part),
            "tp",
            split_axis=2,
            concat_axis=2,
            tiled=True,
        ),
    )
    expert_sum = jnp.sum(expert_pieces.astype(jnp.float32), axis=2).astype(jnp.bfloat16)
    shared_sum = jnp.sum(shared_pieces.astype(jnp.float32), axis=2)[0]
    returned = lax.all_to_all(
        expert_sum.reshape(experts_here, ep_size, capacity, width_part),
        "ep",
        split_axis=1,
        concat_axis=1,
        tiled=True,
    )
    routed = jnp.dot(
        combine,
        returned.reshape(slot_count, width_part).astype(jnp.float32),
        precision=lax.Precision.HIGHEST,
    )
    output = (residual_part.astype(jnp.float32) + shared_sum + routed).astype(jnp.bfloat16)
    new_kv = jnp.concatenate([key_new, value_new], axis=2)
    return (output, new_kv, cum_new)


def solution(mesh):
    in_specs = (
        P("ep", None),
        P("ep"),
        P("ep", None, "tp", None),
        P("ep", "tp", None),
        P(),
        P(None, "tp"),
        P(None, "tp"),
        P(None, "tp"),
        P(None, "tp"),
        P("tp"),
        P("tp", None),
        P(),
        P(None, "tp"),
        P(None, "tp"),
        P("tp", None),
        P("ep", None, "tp"),
        P("ep", None, "tp"),
        P("ep", "tp", None),
        P("ep", None),
        P("ep", None),
    )
    out_specs = (P("ep", "tp"), P("ep", "tp", None), P("ep", "tp"))
    return jax.shard_map(shards, mesh=mesh, in_specs=in_specs, out_specs=out_specs, check_vma=False)
```

profile of v0, /device:TPU:0, one launch (start us, length us, event | category | flops | bytes accessed | tf_op | source)
XLA Modules:
  0.0 160.5 jit_solution(2650859748003632178)
XLA Ops:
  7.2 0.8 broadcast_add_fusion
  8.0 0.7 broadcast_compare_fusion
  8.7 0.7 iota_compare_fusion.3
  9.4 1.0 fusion.23
  10.4 1.6 convolution_convert_fusion.6
  12.4 1.9 %gather_fusion = f32[64]{0:T(128)S(1)} fusion(f32[16,4,768]{2,1,0:T(4,128)} %param.23, s32[64]{0:T(128)S(1)} %reshape.286), kind=kCustom, calls=%fused_computation | custom fusion | bytes 1280 | tf_op jit(solution)/shard_map/jit(take_along_axis)/gather | solution.py:65
  14.5 1.1 fusion.52
  15.7 25.1 %fusion.69 = (bf16[16,768,4,64]{3,2,1,0:T(4,128)(2,1)}, bf16[16,768,4,64]{3,2,1,0:T(4,128)(2,1)}) fusion(bf16[16,768,4,128]{3,2,1,0:T(4,128)(2,1)} %param.22), kind=kLoop, calls=%fused_computation.112 | loop fusion | bytes 25165824 | tf_op jit(solution)/shard_map/slice | solution.py:70
  40.8 0.3 convolution_convert_fusion.5
  41.2 7.9 %fusion.2 = f32[16,4,1,768]{3,2,1,0:T(1,128)S(1)} fusion(bf16[16,4,64,1]{2,3,1,0:T(2,128)(2,1)S(1)} %reshape.299, bf16[16,768,4,64]{3,2,1,0:T(4,128)(2,1)} %get-tuple-element.7), kind=kOutput, calls=%fused_computation.3 | convolution fusion | flops 6291456 | bytes 6496256 | tf_op jit(solution)/shard_map/shd,slhd->shl/dot_general | solution.py:67
  49.9 0.3 convolution_convert_fusion.4
  50.3 6.4 %fusion = f32[16,4,1,64]{3,2,1,0:T(1,128)S(1)} fusion(bf16[16,768,4,64]{3,2,1,0:T(4,128)(2,1)} %get-tuple-element.8, bf16[16,4,768,1]{2,1,0,3:T(4,128)(2,1)S(1)} %fusion.32), kind=kOutput, calls=%fused_computation.1 | convolution fusion | flops 6291456 | bytes 6406144 | tf_op jit(solution)/shard_map/shl,slhd->shd/dot_general | solution.py:87
  56.9 0.9 convolution_convert_fusion.2
  58.7 33.5 %all-reduce.2.cloned.1.call-done = bf16[16,2048]{1,0:T(8,128)(2,1)} async-done(((bf16[16,2048]{1,0:T(8,128)(2,1)}), bf16[16,2048]{1,0:T(8,128)(2,1)}) %all-reduce.2.cloned.1.call-update) | async-done | bytes 65552 | tf_op jit(solution)/shard_map/psum | solution.py:96
  92.2 1.0 fusion.20
  93.5 13.1 %all_to_all.20 = bf16[3,8,8,512]{3,2,0,1:T(8,128)(2,1)S(1)} all-to-all(bf16[3,8,8,512]{3,2,0,1:T(8,128)(2,1)S(1)} %copy.73), channel_id=1, replica_groups=mesh['ep'=8,'tp'=4] {'ep'}, dimensions={1} | all-to-all | bytes 393216 | tf_op jit(solution)/shard_map/all_to_all | solution.py:133
  106.6 7.6 %all_gather.3 = bf16[3,8,8,2048]{3,2,0,1:T(8,128)(2,1)S(1)} all-gather(bf16[3,8,8,512]{3,2,0,1:T(8,128)(2,1)S(1)} %all_to_all.20), channel_id=1, replica_groups=mesh['ep'=8,'tp'=4] {'tp'}, dimensions={3}, use_global_device_ids=true | all-gather | bytes 983040 | tf_op jit(solution)/shard_map/all_gather | solution.py:140
  114.2 1.8 %fusion.10 = f32[3,64,128]{2,1,0:T(8,128)S(1)} fusion(bf16[3,2048,128]{2,1,0:T(8,128)(2,1)} %param.35, bf16[3,8,8,2048]{3,2,0,1:T(8,128)(2,1)S(1)} %all_gather.3), kind=kOutput, calls=%fused_computation.22 | convolution fusion | flops 100663296 | bytes 2457600 | tf_op jit(solution)/shard_map/erd,edf->erf/dot_general | solution.py:143
  116.0 2.0 %convolution_convert_fusion = bf16[3,64,2048]{2,1,0:T(8,128)(2,1)S(1)} fusion(bf16[3,128,2048]{2,1,0:T(8,128)(2,1)S(1)} %copy-done, bf16[3,2048,128]{2,1,0:T(8,128)(2,1)} %param.36, bf16[3,8,8,2048]{3,2,0,1:T(8,128)(2,1)S(1)} %all_gather.3, f32[3,64,128]{2,1,0:T(8,128)S(1)} %fusion.10), kind=kOutput, calls=%fused_computation.5 | convolution fusion | flops 201867264 | bytes 4816896 | tf_op jit(solution)/shard_map/erf,efd->erd/dot_general | solution.py:148
  118.1 1.0 copy.103
  119.0 3.5 %all-to-all-start.2 = ((bf16[3,64,4,512]{3,1,0,2:T(8,128)(2,1)}), bf16[3,64,4,512]{3,1,0,2:T(8,128)(2,1)S(1)}, u32[]{:S(2)}, u32[]{:S(2)}) async-start(bf16[3,64,4,512]{3,1,0,2:T(8,128)(2,1)} %bitcast.49), calls=%async_computation.2 | async-start | bytes 1572864 | tf_op jit(solution)/shard_map/all_to_all | solution.py:152
  122.5 1.2 fusion.70
  123.8 1.5 convolution_convert_fusion.1
  125.4 0.6 copy.66
  126.0 8.1 %all-to-all-done.2 = bf16[3,64,4,512]{3,1,0,2:T(8,128)(2,1)S(1)} async-done(((bf16[3,64,4,512]{3,1,0,2:T(8,128)(2,1)}), bf16[3,64,4,512]{3,1,0,2:T(8,128)(2,1)S(1)}, u32[]{:S(2)}, u32[]{:S(2)}) %all-to-all-start.2) | async-done | bytes 786464 | tf_op jit(solution)/shard_map/all_to_all | solution.py:152
  134.1 3.3 %all-to-all-start = ((bf16[1,16,4,512]{3,1,0,2:T(8,128)(2,1)}), bf16[1,16,4,512]{3,1,0,2:T(8,128)(2,1)S(1)}, u32[]{:S(2)}, u32[]{:S(2)}) async-start(bf16[1,16,4,512]{3,1,0,2:T(8,128)(2,1)} %copy.66), calls=%async_computation | async-start | bytes 131072 | tf_op jit(solution)/shard_map/all_to_all | solution.py:159
  137.6 0.7 copy.76
  138.3 3.2 %all-to-all-done = bf16[1,16,4,512]{3,1,0,2:T(8,128)(2,1)S(1)} async-done(((bf16[1,16,4,512]{3,1,0,2:T(8,128)(2,1)}), bf16[1,16,4,512]{3,1,0,2:T(8,128)(2,1)S(1)}, u32[]{:S(2)}, u32[]{:S(2)}) %all-to-all-start) | async-done | bytes 65568 | tf_op jit(solution)/shard_map/all_to_all | solution.py:159
  141.5 3.4 %all-to-all-start.3 = ((bf16[3,8,8,512]{3,2,0,1:T(8,128)(2,1)}), bf16[3,8,8,512]{3,2,0,1:T(8,128)(2,1)S(1)}, u32[]{:S(2)}, u32[]{:S(2)}) async-start(bf16[3,8,8,512]{3,2,0,1:T(8,128)(2,1)} %copy.76), calls=%async_computation.3 | async-start | bytes 393216 | tf_op jit(solution)/shard_map/all_to_all | solution.py:169
  144.9 0.7 pad_maximum_fusion
  145.7 7.2 %all-to-all-done.3 = bf16[3,8,8,512]{3,2,0,1:T(8,128)(2,1)S(1)} async-done(((bf16[3,8,8,512]{3,2,0,1:T(8,128)(2,1)}), bf16[3,8,8,512]{3,2,0,1:T(8,128)(2,1)S(1)}, u32[]{:S(2)}, u32[]{:S(2)}) %all-to-all-start.3) | async-done | bytes 196640 | tf_op jit(solution)/shard_map/all_to_all | solution.py:169
  152.9 0.8 fusion.5
  (65 shorter events, 3.4 us)
Async XLA Ops:
  7.2 108.9 %copy-start = (bf16[3,128,2048]{2,1,0:T(8,128)(2,1)S(1)}, bf16[3,128,2048]{2,1,0:T(8,128)(2,1)}, u32[]{:S(2)}) copy-start(bf16[3,128,2048]{2,1,0:T(8,128)(2,1)} %param.37) | copy-start | bytes 4718596
  7.2 85.0 %all-reduce.2.cloned.1.call-start = ((), (), s32[]{:S(2)}) async-start(), calls=%async_computation.4 | async-start | bytes 131072 | tf_op jit(solution)/shard_map/psum | solution.py:96
  15.6 25.2 %copy-start.10 = (f32[16,4]{0,1:T(4,128)}, f32[16,4]{0,1:T(4,128)S(1)}, u32[]{:S(2)}) copy-start(f32[16,4]{0,1:T(4,128)S(1)} %fusion.52) | copy-start | bytes 772
  15.6 25.1 %copy-start.2 = (bf16[16,2048]{1,0:T(8,128)(2,1)S(1)}, bf16[16,2048]{1,0:T(8,128)(2,1)}, u32[]{:S(2)}) copy-start(bf16[16,2048]{1,0:T(8,128)(2,1)} %param.20) | copy-start | bytes 196612
  15.7 25.1 %copy-start.3 = (bf16[2048,256]{1,0:T(8,128)(2,1)S(1)}, bf16[2048,256]{1,0:T(8,128)(2,1)}, u32[]{:S(2)}) copy-start(bf16[2048,256]{1,0:T(8,128)(2,1)} %param.26) | copy-start | bytes 3145732
  15.7 25.1 %copy-start.6 = (f32[2048]{0:T(1024)S(1)}, f32[2048]{0:T(1024)}, u32[]{:S(2)}) copy-start(f32[2048]{0:T(1024)} %param.24) | copy-start | bytes 24580
  40.8 8.4 %copy-start.1 = (f32[16,4,768]{2,1,0:T(4,128)S(1)}, f32[16,4,768]{2,1,0:T(4,128)}, u32[]{:S(2)}) copy-start(f32[16,4,768]{2,1,0:T(4,128)} %param.23) | copy-start | bytes 589828
  40.8 9.1 %copy-start.4 = (bf16[2048,256]{1,0:T(8,128)(2,1)S(1)}, bf16[2048,256]{1,0:T(8,128)(2,1)}, u32[]{:S(2)}) copy-start(bf16[2048,256]{1,0:T(8,128)(2,1)} %param.27) | copy-start | bytes 3145732
  50.2 6.7 %copy-start.5 = (bf16[256,2048]{1,0:T(8,128)(2,1)S(1)}, bf16[256,2048]{1,0:T(8,128)(2,1)}, u32[]{:S(2)}) copy-start(bf16[256,2048]{1,0:T(8,128)(2,1)} %param.30) | copy-start | bytes 3145732
  50.3 7.5 %copy-start.8 = (s32[16,6]{0,1:T(8,128)S(1)}, s32[16,6]{0,1:T(8,128)}, u32[]{:S(2)}) copy-start(s32[16,6]{0,1:T(8,128)} %param.38) | copy-start | bytes 1156
  50.3 42.9 %copy-start.7 = (f32[2048]{0:T(1024)S(1)}, f32[2048]{0:T(1024)}, u32[]{:S(2)}) copy-start(f32[2048]{0:T(1024)} %param.31) | copy-start | bytes 24580
  56.7 88.9 %copy-start.9 = (f32[16,6]{0,1:T(8,128)S(1)}, f32[16,6]{0,1:T(8,128)}, u32[]{:S(2)}) copy-start(f32[16,6]{0,1:T(8,128)} %param.39) | copy-start | bytes 1156
  119.0 15.1 %all-to-all-start.2 = ((bf16[3,64,4,512]{3,1,0,2:T(8,128)(2,1)}), bf16[3,64,4,512]{3,1,0,2:T(8,128)(2,1)S(1)}, u32[]{:S(2)}, u32[]{:S(2)}) async-start(bf16[3,64,4,512]{3,1,0,2:T(8,128)(2,1)} %bitcast.49), calls=%async_computation.2 | async-start | bytes 1572864 | tf_op jit(solution)/shard_map/all_to_all | solution.py:152
  134.1 7.4 %all-to-all-start = ((bf16[1,16,4,512]{3,1,0,2:T(8,128)(2,1)}), bf16[1,16,4,512]{3,1,0,2:T(8,128)(2,1)S(1)}, u32[]{:S(2)}, u32[]{:S(2)}) async-start(bf16[1,16,4,512]{3,1,0,2:T(8,128)(2,1)} %copy.66), calls=%async_computation | async-start | bytes 131072 | tf_op jit(solution)/shard_map/all_to_all | solution.py:159
  141.5 11.4 %all-to-all-start.3 = ((bf16[3,8,8,512]{3,2,0,1:T(8,128)(2,1)}), bf16[3,8,8,512]{3,2,0,1:T(8,128)(2,1)S(1)}, u32[]{:S(2)}, u32[]{:S(2)}) async-start(bf16[3,8,8,512]{3,2,0,1:T(8,128)(2,1)} %copy.76), calls=%async_computation.3 | async-start | bytes 393216 | tf_op jit(solution)/shard_map/all_to_all | solution.py:169
Sparse Core Ops, SparseCore 0:
  57.9 34.2 all-reduce.1
where the time goes:
time: 162 us; the launch traced here: 161 us
  waiting for transfers between devices  52.1 us (32%)
  local copies, waits for them, and re-layouts  30.6 us (19%)
  matrix products  26.1 us (16%)
  blocking collectives  20.7 us (13%)
  between operations  14.3 us (9%)
  starting transfers between devices  10.2 us (6%)
  other arithmetic  6.52 us (4%)
    psum x1, waiting for transfers between devices, shards(): lax.psum(partial_value.astype(jnp.bfloat16), 'tp').astype(jnp.float32)  33.5 us
    slice x1, local copies, waits for them, and re-layouts, shards(): cache_kv[:, :, :, :HEAD_DIM]  25.1 us
    all_to_all x1, blocking collectives, shards(): lax.all_to_all(chosen.reshape(experts_here, ep_size, capacity, width_part...  13.1 us
    all_to_all x1, waiting for transfers between devices, shards(): lax.all_to_all(expert_part.reshape(experts_here, row_count, tp_size, widt...  8.13 us
    dot_general x1, matrix products, shards(): jnp.einsum('shd,slhd->shl', queries, cache_kv[:, :, :, :HEAD_DIM], prefer...  7.93 us
    all_gather x1, blocking collectives, shards(): arrived = lax.all_gather(moved, 'tp', axis=3, tiled=True)  7.59 us
    all_to_all x1, waiting for transfers between devices, shards(): lax.all_to_all(expert_sum.reshape(experts_here, ep_size, capacity, width_...  7.17 us
    dot_general x1, matrix products, shards(): jnp.einsum('shl,slhd->shd', probs_past, cache_kv[:, :, :, HEAD_DIM:], pre...  6.38 us
  transfers between devices with their start and end apart: 4, of which 4 were waited for; matrix products, arithmetic and copies ran while one was open for 4% of the time, Pallas kernels for 0%

commit v1 on v0

--- a/solution.py
+++ b/solution.py
@@ -93,7 +93,9 @@
     mixed = mixed + prob_own.astype(jnp.float32)[:, :, None] * value_new.astype(jnp.float32)
     attended = mixed.astype(jnp.bfloat16).reshape(seq_dev, heads_here * HEAD_DIM)
     partial_value = jnp.dot(attended, w_output, preferred_element_type=jnp.float32)
-    summed = lax.psum(partial_value.astype(jnp.bfloat16), "tp").astype(jnp.float32)
+    summed = jnp.sum(lax.all_gather(partial_value.astype(jnp.bfloat16), "tp"), axis=0).astype(
+        jnp.float32
+    )
     residual = (tokens.astype(jnp.float32) + summed).astype(jnp.bfloat16)
     ffn_in = rms_scale(residual, norm_ffn).astype(jnp.bfloat16)
     residual_part = lax.dynamic_slice_in_dim(residual, tp_place * width_part, width_part, 1)

time: 162 us -> 122 us (0.75)
  waiting for transfers between devices: 52.1 us -> 18.5 us
  between operations: 14.3 us -> 0.96 us
  blocking collectives: 20.7 us -> 29.9 us
    psum x1 -> x0, waiting for transfers between devices: 33.5 us -> none  [shards(): lax.psum(partial_value.astype(jnp.bfloat16), 'tp').astype(jnp.float32)]
    all_gather x0 -> x1, blocking collectives: none -> 7.25 us  [shards(): lax.all_gather(partial_value.astype(jnp.bfloat16), 'tp')]
  transfers between devices with their start and end apart: 4 -> 3, of which waited for: 4 -> 3; matrix products, arithmetic and copies ran while one was open for 4% -> 4% of each run, Pallas kernels for 0% -> 0%
where the time goes in v1:
time: 122 us; the launch traced here: 121 us
  local copies, waits for them, and re-layouts  30.6 us (25%)
  blocking collectives  29.9 us (25%)
  matrix products  25.4 us (21%)
  waiting for transfers between devices  18.5 us (15%)
  starting transfers between devices  10.2 us (8%)
  other arithmetic  5.74 us (5%)
    slice x1, local copies, waits for them, and re-layouts, shards(): cache_kv[:, :, :, :HEAD_DIM]  25.1 us
    all_to_all x1, blocking collectives, shards(): lax.all_to_all(chosen.reshape(experts_here, ep_size, capacity, width_part...  14.1 us
    all_gather x1, blocking collectives, shards(): arrived = lax.all_gather(moved, 'tp', axis=3, tiled=True)  8.61 us
    all_to_all x1, waiting for transfers between devices, shards(): lax.all_to_all(expert_part.reshape(experts_here, row_count, tp_size, widt...  8.13 us
    dot_general x1, matrix products, shards(): jnp.einsum('shd,slhd->shl', queries, cache_kv[:, :, :, :HEAD_DIM], prefer...  7.93 us
    all_gather x1, blocking collectives, shards(): lax.all_gather(partial_value.astype(jnp.bfloat16), 'tp')  7.25 us
    all_to_all x1, waiting for transfers between devices, shards(): lax.all_to_all(expert_sum.reshape(experts_here, ep_size, capacity, width_...  7.17 us
    dot_general x1, matrix products, shards(): jnp.einsum('shl,slhd->shd', probs_past, cache_kv[:, :, :, HEAD_DIM:], pre...  6.38 us
  transfers between devices with their start and end apart: 3, of which 3 were waited for; matrix products, arithmetic and copies ran while one was open for 4% of the time, Pallas kernels for 0%

profile of v1, /device:TPU:0, one launch (start us, length us, event | category | flops | bytes accessed | tf_op | source)
XLA Modules:
  0.0 121.4 jit_solution(13317913355612417055)
XLA Ops:
  0.6 0.8 broadcast_add_fusion
  1.4 0.7 broadcast_compare_fusion
  2.1 0.7 iota_compare_fusion.3
  2.8 1.0 fusion.23
  3.8 1.6 %convolution_convert_fusion.6 = bf16[16,256]{1,0:T(8,128)(2,1)S(1)} fusion(bf16[2048,256]{1,0:T(8,128)(2,1)} %param.25, bf16[16,2048]{1,0:T(8,128)(2,1)} %param.20, f32[2048]{0:T(1024)} %param.24, f32[16]{0:T(128)S(1)} %add_rsqrt_fusion.1), kind=kOutput, calls=%fused_computation.15 | convolution fusion | flops 16912384 | bytes 1130560 | tf_op jit(solution)/shard_map/dot_general | solution.py:47
  5.8 1.9 %gather_fusion = f32[64]{0:T(128)S(1)} fusion(f32[16,4,768]{2,1,0:T(4,128)} %param.23, s32[64]{0:T(128)S(1)} %reshape.286), kind=kCustom, calls=%fused_computation | custom fusion | bytes 1280 | tf_op jit(solution)/shard_map/jit(take_along_axis)/gather | solution.py:65
  7.9 1.1 fusion.52
  9.1 25.1 %fusion.69 = (bf16[16,768,4,64]{3,2,1,0:T(4,128)(2,1)}, bf16[16,768,4,64]{3,2,1,0:T(4,128)(2,1)}) fusion(bf16[16,768,4,128]{3,2,1,0:T(4,128)(2,1)} %param.22), kind=kLoop, calls=%fused_computation.112 | loop fusion | bytes 25165824 | tf_op jit(solution)/shard_map/slice | solution.py:70
  34.2 0.3 convolution_convert_fusion.5
  34.6 7.9 %fusion.2 = f32[16,4,1,768]{3,2,1,0:T(1,128)S(1)} fusion(bf16[16,4,64,1]{2,3,1,0:T(2,128)(2,1)S(1)} %reshape.300, bf16[16,768,4,64]{3,2,1,0:T(4,128)(2,1)} %get-tuple-element.7), kind=kOutput, calls=%fused_computation.3 | convolution fusion | flops 6291456 | bytes 6496256 | tf_op jit(solution)/shard_map/shd,slhd->shl/dot_general | solution.py:67
  42.7 0.2 fusion.67
  43.3 0.3 convolution_convert_fusion.4
  43.7 6.4 %fusion = f32[16,4,1,64]{3,2,1,0:T(1,128)S(1)} fusion(bf16[16,768,4,64]{3,2,1,0:T(4,128)(2,1)} %get-tuple-element.8, bf16[16,4,768,1]{2,1,0,3:T(4,128)(2,1)S(1)} %fusion.32), kind=kOutput, calls=%fused_computation.1 | convolution fusion | flops 6291456 | bytes 6406144 | tf_op jit(solution)/shard_map/shl,slhd->shd/dot_general | solution.py:87
  50.3 0.2 convolution_convert_fusion.2
  50.6 7.2 %all-gather = bf16[64,2048]{1,0:T(8,128)(2,1)S(1)} all-gather(bf16[16,2048]{1,0:T(8,128)(2,1)S(1)} %convolution_convert_fusion.2), channel_id=2, replica_groups=mesh['ep'=8,'tp'=4] {'tp'}, dimensions={0}, use_global_device_ids=true | all-gather | bytes 327680 | tf_op jit(solution)/shard_map/all_gather | solution.py:96
  59.2 14.1 %all_to_all.20 = bf16[3,8,8,512]{3,2,0,1:T(8,128)(2,1)S(1)} all-to-all(bf16[3,8,8,512]{3,2,0,1:T(8,128)(2,1)S(1)} %copy.73), channel_id=1, replica_groups=mesh['ep'=8,'tp'=4] {'ep'}, dimensions={1} | all-to-all | bytes 393216 | tf_op jit(solution)/shard_map/all_to_all | solution.py:135
  73.3 8.6 %all_gather.11 = bf16[3,8,8,2048]{3,2,0,1:T(8,128)(2,1)S(1)} all-gather(bf16[3,8,8,512]{3,2,0,1:T(8,128)(2,1)S(1)} %all_to_all.20), channel_id=1, replica_groups=mesh['ep'=8,'tp'=4] {'tp'}, dimensions={3}, use_global_device_ids=true | all-gather | bytes 983040 | tf_op jit(solution)/shard_map/all_gather | solution.py:142
  81.9 1.8 %fusion.10 = f32[3,64,128]{2,1,0:T(8,128)S(1)} fusion(bf16[3,2048,128]{2,1,0:T(8,128)(2,1)} %param.35, bf16[3,8,8,2048]{3,2,0,1:T(8,128)(2,1)S(1)} %all_gather.11), kind=kOutput, calls=%fused_computation.22 | convolution fusion | flops 100663296 | bytes 2457600 | tf_op jit(solution)/shard_map/erd,edf->erf/dot_general | solution.py:145
  83.8 2.0 %convolution_convert_fusion = bf16[3,64,2048]{2,1,0:T(8,128)(2,1)S(1)} fusion(bf16[3,128,2048]{2,1,0:T(8,128)(2,1)S(1)} %copy-done, bf16[3,2048,128]{2,1,0:T(8,128)(2,1)} %param.36, bf16[3,8,8,2048]{3,2,0,1:T(8,128)(2,1)S(1)} %all_gather.11, f32[3,64,128]{2,1,0:T(8,128)S(1)} %fusion.10), kind=kOutput, calls=%fused_computation.5 | convolution fusion | flops 201867264 | bytes 4816896 | tf_op jit(solution)/shard_map/erf,efd->erd/dot_general | solution.py:150
  85.8 1.0 copy.103
  86.8 3.5 %all-to-all-start.2 = ((bf16[3,64,4,512]{3,1,0,2:T(8,128)(2,1)}), bf16[3,64,4,512]{3,1,0,2:T(8,128)(2,1)S(1)}, u32[]{:S(2)}, u32[]{:S(2)}) async-start(bf16[3,64,4,512]{3,1,0,2:T(8,128)(2,1)} %bitcast.50), calls=%async_computation.2 | async-start | bytes 1572864 | tf_op jit(solution)/shard_map/all_to_all | solution.py:154
  90.3 1.2 %fusion.70 = f32[16,128]{1,0:T(8,128)S(1)} fusion(bf16[16,2048]{1,0:T(8,128)(2,1)S(1)} %fusion.22, bf16[2048,128]{1,0:T(8,128)(2,1)} %param.32), kind=kOutput, calls=%fused_computation.113 | convolution fusion | flops 8388608 | bytes 598016 | tf_op jit(solution)/shard_map/dot_general | solution.py:103
  91.5 1.5 %convolution_convert_fusion.1 = bf16[16,2048]{1,0:T(8,128)(2,1)S(1)} fusion(bf16[128,2048]{1,0:T(8,128)(2,1)} %param.34, bf16[16,2048]{1,0:T(8,128)(2,1)S(1)} %fusion.22, bf16[2048,128]{1,0:T(8,128)(2,1)} %param.33, f32[16,128]{1,0:T(8,128)S(1)} %fusion.70), kind=kOutput, calls=%fused_computation.6 | convolution fusion | flops 16822272 | bytes 1187840 | tf_op jit(solution)/shard_map/dot_general | solution.py:106
  93.1 0.6 copy.66
  93.7 8.1 %all-to-all-done.2 = bf16[3,64,4,512]{3,1,0,2:T(8,128)(2,1)S(1)} async-done(((bf16[3,64,4,512]{3,1,0,2:T(8,128)(2,1)}), bf16[3,64,4,512]{3,1,0,2:T(8,128)(2,1)S(1)}, u32[]{:S(2)}, u32[]{:S(2)}) %all-to-all-start.2) | async-done | bytes 786464 | tf_op jit(solution)/shard_map/all_to_all | solution.py:154
  101.8 3.3 %all-to-all-start = ((bf16[1,16,4,512]{3,1,0,2:T(8,128)(2,1)}), bf16[1,16,4,512]{3,1,0,2:T(8,128)(2,1)S(1)}, u32[]{:S(2)}, u32[]{:S(2)}) async-start(bf16[1,16,4,512]{3,1,0,2:T(8,128)(2,1)} %copy.66), calls=%async_computation | async-start | bytes 131072 | tf_op jit(solution)/shard_map/all_to_all | solution.py:161
  105.3 0.7 copy.76
  106.0 3.2 %all-to-all-done = bf16[1,16,4,512]{3,1,0,2:T(8,128)(2,1)S(1)} async-done(((bf16[1,16,4,512]{3,1,0,2:T(8,128)(2,1)}), bf16[1,16,4,512]{3,1,0,2:T(8,128)(2,1)S(1)}, u32[]{:S(2)}, u32[]{:S(2)}) %all-to-all-start) | async-done | bytes 65568 | tf_op jit(solution)/shard_map/all_to_all | solution.py:161
  109.2 3.4 %all-to-all-start.3 = ((bf16[3,8,8,512]{3,2,0,1:T(8,128)(2,1)}), bf16[3,8,8,512]{3,2,0,1:T(8,128)(2,1)S(1)}, u32[]{:S(2)}, u32[]{:S(2)}) async-start(bf16[3,8,8,512]{3,2,0,1:T(8,128)(2,1)} %copy.76), calls=%async_computation.3 | async-start | bytes 393216 | tf_op jit(solution)/shard_map/all_to_all | solution.py:171
  112.6 0.7 pad_maximum_fusion
  113.4 7.2 %all-to-all-done.3 = bf16[3,8,8,512]{3,2,0,1:T(8,128)(2,1)S(1)} async-done(((bf16[3,8,8,512]{3,2,0,1:T(8,128)(2,1)}), bf16[3,8,8,512]{3,2,0,1:T(8,128)(2,1)S(1)}, u32[]{:S(2)}, u32[]{:S(2)}) %all-to-all-start.3) | async-done | bytes 196640 | tf_op jit(solution)/shard_map/all_to_all | solution.py:171
  120.6 0.8 fusion.5
  (64 shorter events, 3.2 us)
Async XLA Ops:
  0.6 83.1 %copy-start = (bf16[3,128,2048]{2,1,0:T(8,128)(2,1)S(1)}, bf16[3,128,2048]{2,1,0:T(8,128)(2,1)}, u32[]{:S(2)}) copy-start(bf16[3,128,2048]{2,1,0:T(8,128)(2,1)} %param.37) | copy-start | bytes 4718596
  9.0 25.2 %copy-start.10 = (f32[16,4]{0,1:T(4,128)}, f32[16,4]{0,1:T(4,128)S(1)}, u32[]{:S(2)}) copy-start(f32[16,4]{0,1:T(4,128)S(1)} %fusion.52) | copy-start | bytes 772
  9.1 25.1 %copy-start.2 = (bf16[16,2048]{1,0:T(8,128)(2,1)S(1)}, bf16[16,2048]{1,0:T(8,128)(2,1)}, u32[]{:S(2)}) copy-start(bf16[16,2048]{1,0:T(8,128)(2,1)} %param.20) | copy-start | bytes 196612
  9.1 25.1 %copy-start.3 = (bf16[2048,256]{1,0:T(8,128)(2,1)S(1)}, bf16[2048,256]{1,0:T(8,128)(2,1)}, u32[]{:S(2)}) copy-start(bf16[2048,256]{1,0:T(8,128)(2,1)} %param.26) | copy-start | bytes 3145732
  9.1 25.1 %copy-start.6 = (f32[2048]{0:T(1024)S(1)}, f32[2048]{0:T(1024)}, u32[]{:S(2)}) copy-start(f32[2048]{0:T(1024)} %param.24) | copy-start | bytes 24580
  34.2 8.4 %copy-start.1 = (f32[16,4,768]{2,1,0:T(4,128)S(1)}, f32[16,4,768]{2,1,0:T(4,128)}, u32[]{:S(2)}) copy-start(f32[16,4,768]{2,1,0:T(4,128)} %param.23) | copy-start | bytes 589828
  34.2 9.1 %copy-start.4 = (bf16[2048,256]{1,0:T(8,128)(2,1)S(1)}, bf16[2048,256]{1,0:T(8,128)(2,1)}, u32[]{:S(2)}) copy-start(bf16[2048,256]{1,0:T(8,128)(2,1)} %param.27) | copy-start | bytes 3145732
  43.6 6.7 %copy-start.5 = (bf16[256,2048]{1,0:T(8,128)(2,1)S(1)}, bf16[256,2048]{1,0:T(8,128)(2,1)}, u32[]{:S(2)}) copy-start(bf16[256,2048]{1,0:T(8,128)(2,1)} %param.30) | copy-start | bytes 3145732
  43.7 14.3 %copy-start.8 = (s32[16,6]{0,1:T(8,128)S(1)}, s32[16,6]{0,1:T(8,128)}, u32[]{:S(2)}) copy-start(s32[16,6]{0,1:T(8,128)} %param.38) | copy-start | bytes 1156
  43.7 15.2 %copy-start.7 = (f32[2048]{0:T(1024)S(1)}, f32[2048]{0:T(1024)}, u32[]{:S(2)}) copy-start(f32[2048]{0:T(1024)} %param.31) | copy-start | bytes 24580
  50.1 63.2 %copy-start.9 = (f32[16,6]{0,1:T(8,128)S(1)}, f32[16,6]{0,1:T(8,128)}, u32[]{:S(2)}) copy-start(f32[16,6]{0,1:T(8,128)} %param.39) | copy-start | bytes 1156
  86.8 15.1 %all-to-all-start.2 = ((bf16[3,64,4,512]{3,1,0,2:T(8,128)(2,1)}), bf16[3,64,4,512]{3,1,0,2:T(8,128)(2,1)S(1)}, u32[]{:S(2)}, u32[]{:S(2)}) async-start(bf16[3,64,4,512]{3,1,0,2:T(8,128)(2,1)} %bitcast.50), calls=%async_computation.2 | async-start | bytes 1572864 | tf_op jit(solution)/shard_map/all_to_all | solution.py:154
  101.8 7.4 %all-to-all-start = ((bf16[1,16,4,512]{3,1,0,2:T(8,128)(2,1)}), bf16[1,16,4,512]{3,1,0,2:T(8,128)(2,1)S(1)}, u32[]{:S(2)}, u32[]{:S(2)}) async-start(bf16[1,16,4,512]{3,1,0,2:T(8,128)(2,1)} %copy.66), calls=%async_computation | async-start | bytes 131072 | tf_op jit(solution)/shard_map/all_to_all | solution.py:161
  109.2 11.4 %all-to-all-start.3 = ((bf16[3,8,8,512]{3,2,0,1:T(8,128)(2,1)}), bf16[3,8,8,512]{3,2,0,1:T(8,128)(2,1)S(1)}, u32[]{:S(2)}, u32[]{:S(2)}) async-start(bf16[3,8,8,512]{3,2,0,1:T(8,128)(2,1)} %copy.76), calls=%async_computation.3 | async-start | bytes 393216 | tf_op jit(solution)/shard_map/all_to_all | solution.py:171
